TPU v7x, 32 devices: a whole 2x2x4 slice. The times are simulated.
32 devices in a mesh: ep: 8 (over z, y), tp: 4 (over x, core).
Axes of the slice: x: 2, y: 2, z: 4, core: 2. Of those that a mesh axis runs over, the one named last changes fastest.
Arguments:
- queries_a: bfloat16 [1024, 1024], P('ep', 'tp'), may hold values from -128 to 128
- queries_b: bfloat16 [1024, 1024], P('ep', 'tp'), may hold values from -128 to 128
- keys_a: bfloat16 [1024, 512], P('ep', 'tp'), may hold values from -8 to 8
- keys_b: bfloat16 [1024, 512], P('ep', 'tp'), may hold values from -8 to 8
- values: bfloat16 [1024, 1024], P('ep', 'tp'), may hold values from -6 to 6
- lambdas: float32 [16], P('tp'), may hold values from 0.3 to 0.8
- head_gain: float32 [128], replicated, may hold values from 0.1 to 1.9
- w_out: bfloat16 [2048, 2048], P('tp'), may hold values from -0.125 to 0.125
- moe_tokens: bfloat16 [4096, 2048], P(('ep', 'tp')), may hold values from -80 to 80
- moe_gain: float32 [2048], replicated, may hold values from 0.1 to 1.9
- routes: int32 [4096, 2], P(('ep', 'tp')), may hold values from 0 to 7, all different within a row; in each aligned block of 128 rows (0 to 127, 128 to 255, ...) at most 48 rows name the same one
- route_weights: float32 [4096, 2], P(('ep', 'tp')), may hold values from 0.1 to 1
- w_gate: bfloat16 [8, 2048, 2048], P('ep', None, 'tp'), may hold values from -4 to 4
- w_up: bfloat16 [8, 2048, 2048], P('ep', None, 'tp'), may hold values from -4 to 4
- w_down: bfloat16 [8, 2048, 2048], P('ep', 'tp'), may hold values from -0.0625 to 0.0625
Outputs:
- mixer_out: bfloat16 [1024, 2048], P(('ep', 'tp'))
- moe_out: bfloat16 [4096, 2048], P(('ep', 'tp'))
Inputs may be any that keep to these rules, and one draw needn't show every extreme that they name: `routes`: each row names 2 different experts. Within the rows of one device no expert is named by more than 48 rows, a bound that some block reaches of some device.
All inputs are finite; a program needn't handle non-finite values.
Results may differ from a plain program's by a relative error of at most 0.011.
Values may be sent and summed in bfloat16 or wider, within the bound.
A program may use at most 192 MiB of HBM per device.

v0:
```python
import jax
import jax.numpy as jnp
from jax import lax
from jax.sharding import PartitionSpec as P

HEAD = 64
VDIM = 128
TOP = 2
eps = 1e-05
alpha_act = 1.702
limit_act = 7.0
negative = -1e30


def clamped_unit(gate, up):
    capped = jnp.minimum(gate, limit_act)
    linear = jnp.clip(up, -limit_act, limit_act)
    return capped * jax.nn.sigmoid(alpha_act * capped) * (linear + 1.0)


def hidden_rows(inputs, gate_matrix, up_matrix):
    gate = jnp.dot(inputs, gate_matrix, preferred_element_type=jnp.float32)
    up = jnp.dot(inputs, up_matrix, preferred_element_type=jnp.float32)
    return clamped_unit(gate, up).astype(jnp.bfloat16)


def pick_rows(table, owner):
    valid = owner < table.shape[0]
    chosen = jnp.take(table, jnp.minimum(owner, table.shape[0] - 1), axis=0)
    return jnp.where(valid[:, None], chosen, jnp.zeros_like(chosen))


def mixer(queries_a, queries_b, keys_a, keys_b, values, lambdas, head_gain, w_out):
    tokens = queries_a.shape[0]
    local_heads = lambdas.shape[0]
    kv_local = keys_a.shape[1] // HEAD
    group = local_heads // kv_local
    scale = HEAD ** (-0.5)
    query_pos = lax.axis_index("ep") * tokens + jnp.arange(tokens, dtype=jnp.int32)
    grouped_a = queries_a.reshape(tokens, kv_local, group, HEAD)
    grouped_b = queries_b.reshape(tokens, kv_local, group, HEAD)
    lowest = jnp.full((kv_local, group, tokens), negative, jnp.float32)
    nothing = jnp.zeros((kv_local, group, tokens), jnp.float32)
    blank = jnp.zeros((kv_local, group, tokens, VDIM), jnp.float32)

    def one_map(grouped, keys, value_rows, visible, state):
        peak, total, accum = state
        scores = (
            jnp.einsum("rgjd,ngd->gjrn", grouped, keys, preferred_element_type=jnp.float32) * scale
        )
        scores = jnp.where(visible, scores, negative)
        new_peak = jnp.maximum(peak, jnp.max(scores, axis=-1))
        expo = jnp.where(visible, jnp.exp(scores - new_peak[..., None]), 0.0)
        total = jnp.sum(expo, axis=-1)
        accum = jnp.einsum(
            "gjrn,ngv->gjrv",
            expo.astype(jnp.bfloat16),
            value_rows,
            preferred_element_type=jnp.float32,
        )
        return (new_peak, total, accum)

    initial = (lowest, nothing, blank, lowest, nothing, blank)
    piece_a = lax.all_gather(keys_a, "ep", axis=0, tiled=True)
    piece_b = lax.all_gather(keys_b, "ep", axis=0, tiled=True)
    piece_v = lax.all_gather(values, "ep", axis=0, tiled=True)
    count = piece_a.shape[0]

    def visit(state):
        key_pos = jnp.arange(count, dtype=jnp.int32)
        visible = key_pos[None, :] <= query_pos[:, None]
        value_rows = piece_v.reshape(count, kv_local, VDIM)
        first = one_map(
            grouped_a, piece_a.reshape(count, kv_local, HEAD), value_rows, visible, state[:3]
        )
        second = one_map(
            grouped_b, piece_b.reshape(count, kv_local, HEAD), value_rows, visible, state[3:]
        )
        return first + second

    result = lax.cond(jnp.int32(0) <= query_pos[tokens - 1], visit, lambda state: state, initial)
    mixed_a = result[2] / result[1][..., None]
    mixed_b = result[5] / result[4][..., None]
    diff = mixed_a - lambdas.reshape(kv_local, group, 1, 1) * mixed_b
    heads_out = (
        diff * lax.rsqrt(jnp.mean(diff * diff, axis=-1, keepdims=True) + eps) * head_gain
    ).astype(jnp.bfloat16)
    weights_out = w_out.reshape(kv_local, group, VDIM, w_out.shape[1])
    return lax.psum_scatter(
        jnp.einsum(
            "gjrv,gjvd->rd", heads_out, weights_out, preferred_element_type=jnp.float32
        ).astype(jnp.bfloat16),
        "tp",
        scatter_dimension=0,
        tiled=True,
    )


def experts(moe_tokens, moe_gain, routes, route_weights, w_gate, w_up, w_down):
    tok_rows, width = moe_tokens.shape
    n_experts = lax.axis_size("ep") * w_gate.shape[0]
    capacity = max(2, 3 * tok_rows * TOP // (2 * n_experts))
    inputs = moe_tokens.astype(jnp.float32)
    normed = (
        inputs * lax.rsqrt(jnp.mean(inputs * inputs, axis=-1, keepdims=True) + eps) * moe_gain
    ).astype(jnp.bfloat16)
    chosen = routes.reshape(-1)
    member = (chosen[:, None] == jnp.arange(n_experts, dtype=jnp.int32)[None, :]).astype(jnp.int32)
    order_in = jnp.sum(jnp.cumsum(member, axis=0) * member, axis=1) - 1
    slot_ids = chosen * capacity + order_in
    owner = (
        jnp.full((n_experts * capacity,), tok_rows, jnp.int32)
        .at[slot_ids]
        .set(jnp.arange(tok_rows * TOP, dtype=jnp.int32) // TOP)
    )
    outgoing = pick_rows(normed, owner).reshape(n_experts, capacity, width)
    arrived = lax.all_to_all(outgoing, "ep", split_axis=0, concat_axis=1, tiled=True).reshape(
        -1, width
    )
    hidden = hidden_rows(lax.all_gather(arrived, "tp", axis=0, tiled=True), w_gate[0], w_up[0])
    expert_out = lax.psum_scatter(
        jnp.dot(hidden, w_down[0], preferred_element_type=jnp.float32).astype(jnp.bfloat16),
        "tp",
        scatter_dimension=0,
        tiled=True,
    )
    returned = lax.all_to_all(
        expert_out.reshape(-1, capacity, width), "ep", split_axis=0, concat_axis=0, tiled=True
    )
    picked = jnp.take(returned.reshape(-1, width), slot_ids, axis=0).reshape(tok_rows, TOP, width)
    return jnp.sum(picked.astype(jnp.float32) * route_weights[:, :, None], axis=1).astype(
        jnp.bfloat16
    )


def body(
    queries_a,
    queries_b,
    keys_a,
    keys_b,
    values,
    lambdas,
    head_gain,
    w_out,
    moe_tokens,
    moe_gain,
    routes,
    route_weights,
    w_gate,
    w_up,
    w_down,
):
    mixer_out = mixer(queries_a, queries_b, keys_a, keys_b, values, lambdas, head_gain, w_out)
    moe_out = experts(moe_tokens, moe_gain, routes, route_weights, w_gate, w_up, w_down)
    return (mixer_out, moe_out)


def solution(mesh):
    return jax.shard_map(
        body,
        mesh=mesh,
        in_specs=(
            P("ep", "tp"),
            P("ep", "tp"),
            P("ep", "tp"),
            P("ep", "tp"),
            P("ep", "tp"),
            P("tp"),
            P(),
            P("tp", None),
            P(("ep", "tp"), None),
            P(),
            P(("ep", "tp"), None),
            P(("ep", "tp"), None),
            P("ep", None, "tp"),
            P("ep", None, "tp"),
            P("ep", "tp", None),
        ),
        out_specs=(P(("ep", "tp"), None), P(("ep", "tp"), None)),
        check_vma=False,
    )
```

profile of v0, /device:TPU:0, one launch (start us, length us, event | category | flops | bytes accessed | tf_op | source)
XLA Modules:
  0.0 350.4 jit_solution(3916929698931288925)
XLA Ops:
  10.3 1.4 scatter_custom_fusion
  12.0 1.2 fusion.27
  13.2 1.2 fusion.29
  14.5 3.1 gather_fusion
  17.6 1.7 select_select_fusion
  19.3 44.2 %all_to_all.14 = bf16[8,48,2048]{2,1,0:T(8,128)(2,1)} all-to-all(bf16[8,48,2048]{2,1,0:T(8,128)(2,1)S(1)} %select_select_fusion), channel_id=1, replica_groups=mesh['ep'=8,'tp'=4] {'ep'}, dimensions={0} | all-to-all | bytes 3145728 | tf_op jit(solution)/shard_map/all_to_all | solution.py:117
  63.5 45.5 %all-gather.2.cloned.1.call-done = bf16[1536,2048]{1,0:T(8,128)(2,1)} async-done(((bf16[384,2048]{1,0:T(8,128)(2,1)}), bf16[1536,2048]{1,0:T(8,128)(2,1)}) %all-gather.2.cloned.1.call-update) | async-done | bytes 6291472 | tf_op jit(solution)/shard_map/all_gather | solution.py:120
  109.0 8.5 %convolution_minimum_fusion = f32[1536,512]{1,0:T(8,128)} fusion(bf16[1536,2048]{1,0:T(8,128)(2,1)} %all-gather.2.cloned.1.call-done, bf16[1,2048,512]{2,1,0:T(8,128)(2,1)} %param.29), kind=kOutput, calls=%fused_computation.30 | convolution fusion | flops 3222011904 | bytes 11534336 | tf_op jit(solution)/shard_map/dot_general | solution.py:22
  117.5 11.9 %convolution_convert_fusion = bf16[1536,2048]{1,0:T(8,128)(2,1)} fusion(bf16[1,512,2048]{2,1,0:T(8,128)(2,1)S(1)} %copy-done, bf16[1536,2048]{1,0:T(8,128)(2,1)} %all-gather.2.cloned.1.call-done, f32[1536,512]{1,0:T(8,128)} %convolution_minimum_fusion, bf16[1,2048,512]{2,1,0:T(8,128)(2,1)} %param.30), kind=kOutput, calls=%fused_computation.28 | convolution fusion | flops 6452674560 | bytes 19922944 | tf_op jit(solution)/shard_map/dot_general | solution.py:122
  129.5 58.9 %reduce-scatter.5.cloned.1.call-done = bf16[384,2048]{1,0:T(8,128)(2,1)} async-done(((bf16[1536,2048]{1,0:T(8,128)(2,1)}), bf16[384,2048]{1,0:T(8,128)(2,1)}) %reduce-scatter.5.cloned.1.call-update) | async-done | bytes 1572880 | tf_op jit(solution)/shard_map/reduce_scatter | solution.py:121
  188.4 5.5 %all-to-all-start.1 = ((bf16[8,48,2048]{2,1,0:T(8,128)(2,1)}), bf16[8,48,2048]{2,1,0:T(8,128)(2,1)}, u32[]{:S(2)}, u32[]{:S(2)}) async-start(bf16[8,48,2048]{2,1,0:T(8,128)(2,1)} %bitcast.77), calls=%async_computation.3 | async-start | bytes 3145728 | tf_op jit(solution)/shard_map/all_to_all | solution.py:127
  196.2 54.2 %all_gather.12 = bf16[1024,128]{0,1:T(8,128)(2,1)S(1)} all-gather(bf16[128,128]{0,1:T(8,128)(2,1)S(1)} %copy.45), channel_id=1, replica_groups=mesh['ep'=8,'tp'=4] {'ep'}, dimensions={0}, use_global_device_ids=true | all-gather | bytes 294912 | tf_op jit(solution)/shard_map/all_gather | solution.py:64
  250.3 27.8 %all_gather.14 = bf16[1024,128]{0,1:T(8,128)(2,1)} all-gather(bf16[128,128]{0,1:T(8,128)(2,1)S(1)} %copy.46), channel_id=1, replica_groups=mesh['ep'=8,'tp'=4] {'ep'}, dimensions={0}, use_global_device_ids=true | all-gather | bytes 294912 | tf_op jit(solution)/shard_map/all_gather | solution.py:65
  278.2 31.3 %all_gather.13 = bf16[1024,256]{1,0:T(8,128)(2,1)S(1)} all-gather(bf16[128,256]{1,0:T(8,128)(2,1)S(1)} %copy-done.6), channel_id=1, replica_groups=mesh['ep'=8,'tp'=4] {'ep'}, dimensions={0}, use_global_device_ids=true | all-gather | bytes 589824 | tf_op jit(solution)/shard_map/all_gather | solution.py:66
  309.5 12.2 %conditional.1 = (f32[2,2,128]{2,1,0:T(2,128)S(1)}, f32[2,2,128,128]{3,2,1,0:T(8,128)S(1)}, f32[2,2,128]{2,1,0:T(2,128)S(1)}, f32[2,2,128,128]{3,2,1,0:T(8,128)S(1)}) conditional(s32[]{:T(128)} %bitcast.12, () %tuple.16, (s32[128]{0:T(128)S(1)}, bf16[1024,128]{0,1:T(8,128)(2,1)S(1)}, bf16[128,256]{1,0:T(8,128)(2,1)}, bf16[1024,256]{1,0:T(8,128)(2,1)S(1)}, ...), branch_computations={%region_0.0_spmd, %region_1.6_spmd} | conditional | flops 416414720 | bytes 47481572 | solution.py:81
  310.6 1.8 fusion.42
  312.5 2.4 fusion.1
  317.2 2.6 fusion.6
  319.8 1.9 fusion.8
  322.7 2.9 fusion.23
  326.2 4.0 %gather_fusion.1 = bf16[256,2048]{1,0:T(8,128)(2,1)S(1)} fusion(bf16[384,2048]{1,0:T(8,128)(2,1)} %bitcast.26, s32[1024]{0:T(1024)S(1)} %pad_clamp_fusion), kind=kCustom, calls=%fused_computation.1 | custom fusion | bytes 2098176 | tf_op jit(solution)/shard_map/jit(_take)/gather | solution.py:130
  330.2 1.5 gather.15
  331.7 6.2 %multiply_reduce_fusion = bf16[128,2048]{1,0:T(8,128)(2,1)} fusion(bf16[128,2,2048]{2,1,0:T(2,128)(2,1)} %gather.15, pred[128,2]{1,0:T(8,128)(4,1)S(1)} %copy.52, f32[128,2]{1,0:T(8,128)S(1)} %copy.54), kind=kLoop, calls=%fused_computation.39 | loop fusion | flops 1835008 | bytes 1574144 | tf_op jit(solution)/shard_map/reduce_sum | solution.py:131
  338.0 5.9 %reduce-scatter.3.cloned.1.call-done = bf16[32,2048]{1,0:T(8,128)(2,1)} async-done(((bf16[128,2048]{1,0:T(8,128)(2,1)}), bf16[32,2048]{1,0:T(8,128)(2,1)}) %reduce-scatter.3.cloned.1.call-update) | async-done | bytes 131088 | tf_op jit(solution)/shard_map/reduce_scatter | solution.py:89
  (79 shorter events, 9.8 us)
Async XLA Ops:
  7.2 110.4 %copy-start = (bf16[1,512,2048]{2,1,0:T(8,128)(2,1)S(1)}, bf16[1,512,2048]{2,1,0:T(8,128)(2,1)}, u32[]{:S(2)}) copy-start(bf16[1,512,2048]{2,1,0:T(8,128)(2,1)} %param.31) | copy-start | bytes 6291460
  7.2 101.8 %all-gather.2.cloned.1.call-start = ((), (), s32[]{:S(2)}) async-start(), calls=%async_computation.5 | async-start | bytes 7864320 | tf_op jit(solution)/shard_map/all_gather | solution.py:120
  10.3 1.4 copy-start.12
  63.5 124.9 %reduce-scatter.5.cloned.1.call-start = ((), (), s32[]{:S(2)}) async-start(), calls=%async_computation.6 | async-start | bytes 7864320 | tf_op jit(solution)/shard_map/reduce_scatter | solution.py:121
  129.4 64.6 %copy-start.8 = (bf16[128,128]{1,0:T(8,128)(2,1)S(1)}, bf16[128,128]{1,0:T(8,128)(2,1)}, u32[]{:S(2)}) copy-start(bf16[128,128]{1,0:T(8,128)(2,1)} %param.19) | copy-start | bytes 98308
  129.4 64.7 %copy-start.9 = (bf16[128,128]{1,0:T(8,128)(2,1)S(1)}, bf16[128,128]{1,0:T(8,128)(2,1)}, u32[]{:S(2)}) copy-start(bf16[128,128]{1,0:T(8,128)(2,1)} %param.20) | copy-start | bytes 98308
  129.5 66.0 %copy-start.15 = (f32[4]{0:T(128)S(1)}, f32[4]{0:T(128)}, u32[]{:S(2)}) copy-start(f32[4]{0:T(128)} %param.22) | copy-start | bytes 52
  129.5 148.7 %copy-start.6 = (bf16[128,256]{1,0:T(8,128)(2,1)S(1)}, bf16[128,256]{1,0:T(8,128)(2,1)}, u32[]{:S(2)}) copy-start(bf16[128,256]{1,0:T(8,128)(2,1)} %param.21) | copy-start | bytes 196612
  188.4 137.8 %all-to-all-start.1 = ((bf16[8,48,2048]{2,1,0:T(8,128)(2,1)}), bf16[8,48,2048]{2,1,0:T(8,128)(2,1)}, u32[]{:S(2)}, u32[]{:S(2)}) async-start(bf16[8,48,2048]{2,1,0:T(8,128)(2,1)} %bitcast.77), calls=%async_computation.3 | async-start | bytes 3145728 | tf_op jit(solution)/shard_map/all_to_all | solution.py:127
  193.9 149.9 %reduce-scatter.3.cloned.1.call-start = ((), (), s32[]{:S(2)}) async-start(), calls=%async_computation.4 | async-start | bytes 655360 | tf_op jit(solution)/shard_map/reduce_scatter | solution.py:89
  309.5 2.9 copy-start.7
  309.5 3.0 copy-start.4
  312.5 2.5 copy-start.1
  315.0 1.3 copy-start.3
  315.0 1.3 copy-start.11
  316.4 0.8 copy-start.5
  317.2 2.6 copy-start.2
  321.7 4.2 %copy-start.10 = (s32[128,2]{0,1:T(2,128)S(1)}, s32[128,2]{0,1:T(2,128)}, u32[]{:S(2)}) copy-start(s32[128,2]{0,1:T(2,128)} %param.27) | copy-start | bytes 3076
  321.7 4.4 %copy-start.14 = (f32[128,2]{0,1:T(2,128)S(1)}, f32[128,2]{0,1:T(2,128)}, u32[]{:S(2)}) copy-start(f32[128,2]{0,1:T(2,128)} %param.28) | copy-start | bytes 3076
  321.7 4.5 %copy-start.13 = (s32[256,1]{0,1:T(1,128)S(1)}, s32[256,1]{0,1:T(1,128)}, u32[]{:S(2)}) copy-start(s32[256,1]{0,1:T(1,128)} %copy-done.12) | copy-start | bytes 3076
Sparse Core Ops, SparseCore 0:
  63.6 45.3 all-gather.1
  129.6 58.8 reduce-scatter.4
  325.8 18.0 reduce-scatter.2
where the time goes:
time: 351 us; the launch traced here: 350 us
  blocking collectives  158 us (45%)
  waiting for transfers between devices  110 us (31%)
  matrix products  32.1 us (9%)
  local copies, waits for them, and re-layouts  16.1 us (5%)
  between operations  14.7 us (4%)
  other arithmetic  14 us (4%)
  starting transfers between devices  5.63 us (2%)
    reduce_scatter x1, waiting for transfers between devices, experts(): lax.psum_scatter(jnp.dot(hidden, w_down[0], preferred_element_type=jnp.fl...  58.9 us
    all_gather x1, blocking collectives, mixer(): piece_a = lax.all_gather(keys_a, 'ep', axis=0, tiled=True)  54.2 us
    all_gather x1, waiting for transfers between devices, experts(): lax.all_gather(arrived, 'tp', axis=0, tiled=True)  45.5 us
    all_to_all x1, blocking collectives, experts(): lax.all_to_all(outgoing, 'ep', split_axis=0, concat_axis=1, tiled=True)  44.2 us
    all_gather x1, blocking collectives, mixer(): piece_v = lax.all_gather(values, 'ep', axis=0, tiled=True)  31.3 us
    all_gather x1, blocking collectives, mixer(): piece_b = lax.all_gather(keys_b, 'ep', axis=0, tiled=True)  27.8 us
    dot_general x1, matrix products, experts(): jnp.dot(hidden, w_down[0], preferred_element_type=jnp.float32)  11.9 us
    dot_general x1, matrix products, hidden_rows(): gate = jnp.dot(inputs, gate_matrix, preferred_element_type=jnp.float32)  8.52 us
  transfers between devices with their start and end apart: 4, of which 3 were waited for; matrix products, arithmetic and copies ran while one was open for 8% of the time, Pallas kernels for 0%

commit v1 on v0

--- a/solution.py
+++ b/solution.py
@@ -114,9 +114,10 @@
         .set(jnp.arange(tok_rows * TOP, dtype=jnp.int32) // TOP)
     )
     outgoing = pick_rows(normed, owner).reshape(n_experts, capacity, width)
-    arrived = lax.all_to_all(outgoing, "ep", split_axis=0, concat_axis=1, tiled=True).reshape(
-        -1, width
-    )
+    arrived = jnp.concatenate(
+        lax.all_to_all(jnp.stack(jnp.split(outgoing, lax.axis_size("ep"), axis=0)), "ep", 0, 0),
+        axis=1,
+    ).reshape(-1, width)
     hidden = hidden_rows(lax.all_gather(arrived, "tp", axis=0, tiled=True), w_gate[0], w_up[0])
     expert_out = lax.psum_scatter(
         jnp.dot(hidden, w_down[0], preferred_element_type=jnp.float32).astype(jnp.bfloat16),

time: 351 us -> 351 us (level)
  no operation moved by 1% of the time
where the time goes in v1:
time: 351 us; the launch traced here: 350 us
  blocking collectives  158 us (45%)
  waiting for transfers between devices  110 us (31%)
  matrix products  32.1 us (9%)
  local copies, waits for them, and re-layouts  16.1 us (5%)
  between operations  14.7 us (4%)
  other arithmetic  14 us (4%)
  starting transfers between devices  5.63 us (2%)
    reduce_scatter x1, waiting for transfers between devices, experts(): lax.psum_scatter(jnp.dot(hidden, w_down[0], preferred_element_type=jnp.fl...  59 us
    all_gather x1, blocking collectives, mixer(): piece_a = lax.all_gather(keys_a, 'ep', axis=0, tiled=True)  54.2 us
    all_gather x1, waiting for transfers between devices, experts(): lax.all_gather(arrived, 'tp', axis=0, tiled=True)  45.5 us
    all_to_all x1, blocking collectives, experts(): lax.all_to_all(jnp.stack(jnp.split(outgoing, lax.axis_size('ep'), axis=0)...  44.2 us
    all_gather x1, blocking collectives, mixer(): piece_v = lax.all_gather(values, 'ep', axis=0, tiled=True)  31.3 us
    all_gather x1, blocking collectives, mixer(): piece_b = lax.all_gather(keys_b, 'ep', axis=0, tiled=True)  27.8 us
    dot_general x1, matrix products, experts(): jnp.dot(hidden, w_down[0], preferred_element_type=jnp.float32)  11.9 us
    dot_general x1, matrix products, hidden_rows(): gate = jnp.dot(inputs, gate_matrix, preferred_element_type=jnp.float32)  8.52 us
  transfers between devices with their start and end apart: 4, of which 3 were waited for; matrix products, arithmetic and copies ran while one was open for 8% of the time, Pallas kernels for 0%

profile of v1, /device:TPU:0, one launch (start us, length us, event | category | flops | bytes accessed | tf_op | source)
XLA Modules:
  0.0 350.5 jit_solution(1431430407252617084)
XLA Ops:
  10.3 1.4 scatter_custom_fusion
  11.8 1.2 fusion.27
  13.0 1.2 fusion.29
  14.3 3.1 gather_fusion
  17.4 1.7 select_select_fusion
  19.3 44.2 %all_to_all.10 = bf16[8,1,48,2048]{3,2,1,0:T(8,128)(2,1)} all-to-all(bf16[8,1,48,2048]{3,2,1,0:T(8,128)(2,1)S(1)} %fusion.32), channel_id=1, replica_groups=mesh['ep'=8,'tp'=4] {'ep'}, dimensions={0} | all-to-all | bytes 3145728 | tf_op jit(solution)/shard_map/all_to_all | solution.py:118
  63.6 45.5 %all-gather.2.cloned.1.call-done = bf16[1536,2048]{1,0:T(8,128)(2,1)} async-done(((bf16[384,2048]{1,0:T(8,128)(2,1)}), bf16[1536,2048]{1,0:T(8,128)(2,1)}) %all-gather.2.cloned.1.call-update) | async-done | bytes 6291472 | tf_op jit(solution)/shard_map/all_gather | solution.py:121
  109.0 8.5 %convolution_minimum_fusion = f32[1536,512]{1,0:T(8,128)} fusion(bf16[1536,2048]{1,0:T(8,128)(2,1)} %all-gather.2.cloned.1.call-done, bf16[1,2048,512]{2,1,0:T(8,128)(2,1)} %param.29), kind=kOutput, calls=%fused_computation.30 | convolution fusion | flops 3222011904 | bytes 11534336 | tf_op jit(solution)/shard_map/dot_general | solution.py:22
  117.6 11.9 %convolution_convert_fusion = bf16[1536,2048]{1,0:T(8,128)(2,1)} fusion(bf16[1,512,2048]{2,1,0:T(8,128)(2,1)S(1)} %copy-done, bf16[1536,2048]{1,0:T(8,128)(2,1)} %all-gather.2.cloned.1.call-done, f32[1536,512]{1,0:T(8,128)} %convolution_minimum_fusion, bf16[1,2048,512]{2,1,0:T(8,128)(2,1)} %param.30), kind=kOutput, calls=%fused_computation.28 | convolution fusion | flops 6452674560 | bytes 19922944 | tf_op jit(solution)/shard_map/dot_general | solution.py:123
  129.5 59.0 %reduce-scatter.5.cloned.1.call-done = bf16[384,2048]{1,0:T(8,128)(2,1)} async-done(((bf16[1536,2048]{1,0:T(8,128)(2,1)}), bf16[384,2048]{1,0:T(8,128)(2,1)}) %reduce-scatter.5.cloned.1.call-update) | async-done | bytes 1572880 | tf_op jit(solution)/shard_map/reduce_scatter | solution.py:122
  188.5 5.5 %all-to-all-start.1 = ((bf16[8,48,2048]{2,1,0:T(8,128)(2,1)}), bf16[8,48,2048]{2,1,0:T(8,128)(2,1)}, u32[]{:S(2)}, u32[]{:S(2)}) async-start(bf16[8,48,2048]{2,1,0:T(8,128)(2,1)} %bitcast.107), calls=%async_computation.3 | async-start | bytes 3145728 | tf_op jit(solution)/shard_map/all_to_all | solution.py:128
  196.2 54.2 %all_gather.12 = bf16[1024,128]{0,1:T(8,128)(2,1)S(1)} all-gather(bf16[128,128]{0,1:T(8,128)(2,1)S(1)} %copy.45), channel_id=1, replica_groups=mesh['ep'=8,'tp'=4] {'ep'}, dimensions={0}, use_global_device_ids=true | all-gather | bytes 294912 | tf_op jit(solution)/shard_map/all_gather | solution.py:64
  250.4 27.8 %all_gather.14 = bf16[1024,128]{0,1:T(8,128)(2,1)} all-gather(bf16[128,128]{0,1:T(8,128)(2,1)S(1)} %copy.46), channel_id=1, replica_groups=mesh['ep'=8,'tp'=4] {'ep'}, dimensions={0}, use_global_device_ids=true | all-gather | bytes 294912 | tf_op jit(solution)/shard_map/all_gather | solution.py:65
  278.2 31.3 %all_gather.13 = bf16[1024,256]{1,0:T(8,128)(2,1)S(1)} all-gather(bf16[128,256]{1,0:T(8,128)(2,1)S(1)} %copy-done.6), channel_id=1, replica_groups=mesh['ep'=8,'tp'=4] {'ep'}, dimensions={0}, use_global_device_ids=true | all-gather | bytes 589824 | tf_op jit(solution)/shard_map/all_gather | solution.py:66
  309.5 12.2 %conditional.1 = (f32[2,2,128]{2,1,0:T(2,128)S(1)}, f32[2,2,128,128]{3,2,1,0:T(8,128)S(1)}, f32[2,2,128]{2,1,0:T(2,128)S(1)}, f32[2,2,128,128]{3,2,1,0:T(8,128)S(1)}) conditional(s32[]{:T(128)} %bitcast.12, () %tuple.16, (s32[128]{0:T(128)S(1)}, bf16[1024,128]{0,1:T(8,128)(2,1)S(1)}, bf16[128,256]{1,0:T(8,128)(2,1)}, bf16[1024,256]{1,0:T(8,128)(2,1)S(1)}, ...), branch_computations={%region_0.0_spmd, %region_1.6_spmd} | conditional | flops 416414720 | bytes 47481572 | solution.py:81
  310.6 1.8 fusion.50
  312.6 2.4 fusion.1
  317.2 2.6 fusion.6
  319.8 1.9 fusion.8
  322.8 2.9 fusion.23
  326.3 4.0 %gather_fusion.1 = bf16[256,2048]{1,0:T(8,128)(2,1)S(1)} fusion(bf16[384,2048]{1,0:T(8,128)(2,1)} %bitcast.33, s32[1024]{0:T(1024)S(1)} %pad_clamp_fusion), kind=kCustom, calls=%fused_computation.1 | custom fusion | bytes 2098176 | tf_op jit(solution)/shard_map/jit(_take)/gather | solution.py:131
  330.3 1.5 gather.12
  331.8 6.2 %multiply_reduce_fusion = bf16[128,2048]{1,0:T(8,128)(2,1)} fusion(bf16[128,2,2048]{2,1,0:T(2,128)(2,1)} %gather.12, pred[128,2]{1,0:T(8,128)(4,1)S(1)} %copy.52, f32[128,2]{1,0:T(8,128)S(1)} %copy.54), kind=kLoop, calls=%fused_computation.39 | loop fusion | flops 1835008 | bytes 1574144 | tf_op jit(solution)/shard_map/reduce_sum | solution.py:132
  338.0 5.9 %reduce-scatter.3.cloned.1.call-done = bf16[32,2048]{1,0:T(8,128)(2,1)} async-done(((bf16[128,2048]{1,0:T(8,128)(2,1)}), bf16[32,2048]{1,0:T(8,128)(2,1)}) %reduce-scatter.3.cloned.1.call-update) | async-done | bytes 131088 | tf_op jit(solution)/shard_map/reduce_scatter | solution.py:89
  (85 shorter events, 9.8 us)
Async XLA Ops:
  7.2 110.4 %copy-start = (bf16[1,512,2048]{2,1,0:T(8,128)(2,1)S(1)}, bf16[1,512,2048]{2,1,0:T(8,128)(2,1)}, u32[]{:S(2)}) copy-start(bf16[1,512,2048]{2,1,0:T(8,128)(2,1)} %param.31) | copy-start | bytes 6291460
  7.2 101.8 %all-gather.2.cloned.1.call-start = ((), (), s32[]{:S(2)}) async-start(), calls=%async_computation.5 | async-start | bytes 7864320 | tf_op jit(solution)/shard_map/all_gather | solution.py:121
  10.3 1.4 copy-start.12
  63.5 125.0 %reduce-scatter.5.cloned.1.call-start = ((), (), s32[]{:S(2)}) async-start(), calls=%async_computation.6 | async-start | bytes 7864320 | tf_op jit(solution)/shard_map/reduce_scatter | solution.py:122
  129.4 64.6 %copy-start.8 = (bf16[128,128]{1,0:T(8,128)(2,1)S(1)}, bf16[128,128]{1,0:T(8,128)(2,1)}, u32[]{:S(2)}) copy-start(bf16[128,128]{1,0:T(8,128)(2,1)} %param.19) | copy-start | bytes 98308
  129.5 64.7 %copy-start.9 = (bf16[128,128]{1,0:T(8,128)(2,1)S(1)}, bf16[128,128]{1,0:T(8,128)(2,1)}, u32[]{:S(2)}) copy-start(bf16[128,128]{1,0:T(8,128)(2,1)} %param.20) | copy-start | bytes 98308
  129.5 66.1 %copy-start.15 = (f32[4]{0:T(128)S(1)}, f32[4]{0:T(128)}, u32[]{:S(2)}) copy-start(f32[4]{0:T(128)} %param.22) | copy-start | bytes 52
  129.5 148.7 %copy-start.6 = (bf16[128,256]{1,0:T(8,128)(2,1)S(1)}, bf16[128,256]{1,0:T(8,128)(2,1)}, u32[]{:S(2)}) copy-start(bf16[128,256]{1,0:T(8,128)(2,1)} %param.21) | copy-start | bytes 196612
  188.5 137.8 %all-to-all-start.1 = ((bf16[8,48,2048]{2,1,0:T(8,128)(2,1)}), bf16[8,48,2048]{2,1,0:T(8,128)(2,1)}, u32[]{:S(2)}, u32[]{:S(2)}) async-start(bf16[8,48,2048]{2,1,0:T(8,128)(2,1)} %bitcast.107), calls=%async_computation.3 | async-start | bytes 3145728 | tf_op jit(solution)/shard_map/all_to_all | solution.py:128
  194.0 149.9 %reduce-scatter.3.cloned.1.call-start = ((), (), s32[]{:S(2)}) async-start(), calls=%async_computation.4 | async-start | bytes 655360 | tf_op jit(solution)/shard_map/reduce_scatter | solution.py:89
  309.5 2.9 copy-start.7
  309.5 3.1 copy-start.4
  312.6 2.5 copy-start.1
  315.0 1.3 copy-start.3
  315.0 1.3 copy-start.11
  316.4 0.8 copy-start.5
  317.2 2.6 copy-start.2
  321.7 4.2 %copy-start.10 = (s32[128,2]{0,1:T(2,128)S(1)}, s32[128,2]{0,1:T(2,128)}, u32[]{:S(2)}) copy-start(s32[128,2]{0,1:T(2,128)} %param.27) | copy-start | bytes 3076
  321.8 4.4 %copy-start.14 = (f32[128,2]{0,1:T(2,128)S(1)}, f32[128,2]{0,1:T(2,128)}, u32[]{:S(2)}) copy-start(f32[128,2]{0,1:T(2,128)} %param.28) | copy-start | bytes 3076
  321.8 4.5 %copy-start.13 = (s32[256,1]{0,1:T(1,128)S(1)}, s32[256,1]{0,1:T(1,128)}, u32[]{:S(2)}) copy-start(s32[256,1]{0,1:T(1,128)} %copy-done.12) | copy-start | bytes 3076
Sparse Core Ops, SparseCore 0:
  63.6 45.3 all-gather.1
  129.6 58.8 reduce-scatter.4
  325.9 18.0 reduce-scatter.2
